TPU v7x, 512 devices: a whole 4x8x8 slice. The times are simulated.
512 devices in a mesh: ep: 32 (over z, x), tp: 16 (over y, core).
Axes of the slice: x: 4, y: 8, z: 8, core: 2. Of those that a mesh axis runs over, the one named last changes fastest.
Arguments:
- mixer_in: bfloat16 [4096, 2048], P('ep'), may hold values from -6 to 6
- mixer_gain: float32 [2048], replicated, may hold values from 0.1 to 1.9
- w_value: bfloat16 [2048, 1536], P(None, 'tp'), may hold values from -0.125 to 0.125
- w_gate: bfloat16 [2048, 1536], P(None, 'tp'), may hold values from -0.125 to 0.125
- w_taps: float32 [31, 1536], P(None, 'tp'), may hold values from -3 to 3
- channel_gain: float32 [1536], P('tp'), may hold values from 0.1 to 1.9
- w_output: bfloat16 [1536, 2048], P('tp'), may hold values from -0.15625 to 0.15625
- expert_in: bfloat16 [4096, 2048], P('ep'), may hold values from -6 to 6
- expert_gain: float32 [2048], replicated, may hold values from 0 to 8
- route_experts: int32 [4096, 4], P('ep'), may hold values from 0 to 31, all different within a row; in each aligned block of 128 rows (0 to 127, 128 to 255, ...) at most 32 rows name the same one
- route_scores: float32 [4096, 4], P('ep'), may hold values from -6 to 6
- expert_gate: bfloat16 [32, 2048, 2048], P('ep', None, 'tp'), may hold values from -0.125 to 0.125
- expert_up: bfloat16 [32, 2048, 2048], P('ep', None, 'tp'), may hold values from -0.125 to 0.125
- expert_down: bfloat16 [32, 2048, 2048], P('ep', 'tp'), may hold values from -0.125 to 0.125
Outputs:
- mixer_out: bfloat16 [4096, 2048], P('ep')
- expert_out: bfloat16 [4096, 2048], P('ep')
Inputs may be any that keep to these rules, and one draw needn't show every extreme that they name: `route_experts`: each row names 4 different experts. In each aligned block of 128 rows (the rows of one index of ep) no expert is named more than 32 times, a bound that some block reaches.
All inputs are finite; a program needn't handle non-finite values.
Results may differ from a plain program's by a relative error of at most 0.02.
Values may be sent and summed in bfloat16 or wider, within the bound.
No kernel may reach another device: no remote copies, remote signals or barrier semaphores. Data moves between devices by JAX's collectives and lax.ppermute only.
A program may use at most 64 MiB of HBM per device.

v0:
```python
import jax
import jax.numpy as jnp
from jax import lax
from jax.sharding import Mesh
from jax.sharding import PartitionSpec as P

CONV_CH = 1536
CONV_W = 31
TOP_K = 4
TP = ("tp_0", "tp_1")
epsilon = 1e-05
clamp_limit = 7.0
swish_slope = 1.702


def shifted(block, axis, distance):
    devices = range(lax.axis_size(axis))
    route = [(i - distance, i) for i in devices if i - distance in devices]
    return lax.ppermute(block, axis, route)


def sent_to_all(x, axis):
    copies = jnp.broadcast_to(x, (lax.axis_size(axis), *x.shape))
    return lax.all_to_all(copies, axis, split_axis=0, concat_axis=0, tiled=True)


def over_copies(x, axis):
    everything = sent_to_all(x, axis)
    return jnp.sum(everything, axis=0)


def packed_total(arrays, axis):
    line, at, done = (jnp.concatenate([a.reshape(-1) for a in arrays]), 0, [])
    subtotal = over_copies(line, axis)
    for a in arrays:
        done.append(subtotal[at : at + a.size].reshape(a.shape))
        at += a.size
    return tuple(done)


def by_axis(x, axes):
    for axis in axes:
        x = lax.psum(x, axis)
    return x


def row_norm(inputs, gains):
    widened = inputs.astype(jnp.float32)
    row_mean = jnp.mean(widened, axis=-1, keepdims=True)
    row_var = jnp.mean(jnp.square(widened - row_mean), axis=-1, keepdims=True)
    return (widened - row_mean) * lax.rsqrt(row_var + epsilon) * gains


def local(
    mixer_in,
    mixer_gain,
    w_value,
    w_gate,
    w_taps,
    channel_gain,
    w_output,
    expert_in,
    expert_gain,
    route_experts,
    route_scores,
    expert_gate,
    expert_up,
    expert_down,
):
    normed = row_norm(mixer_in, mixer_gain).astype(jnp.bfloat16)
    values = jnp.dot(normed, w_value, preferred_element_type=jnp.float32)
    gate_pre = jnp.dot(normed, w_gate, preferred_element_type=jnp.float32)
    gated_values = (values * jax.nn.sigmoid(gate_pre)).astype(jnp.bfloat16)
    mixer_rows = gated_values.shape[0]
    reach_rows = CONV_W - 1
    earlier = shifted(gated_values[mixer_rows - reach_rows :], "ep", 1)
    extended = jnp.concatenate([earlier, gated_values], axis=0)
    conv_out = jnp.zeros(gated_values.shape, jnp.float32)
    for offset in range(CONV_W):
        conv_out = (
            conv_out + extended[offset : offset + mixer_rows].astype(jnp.float32) * w_taps[offset]
        )
    channel_sums = packed_total(
        (
            jnp.sum(conv_out, axis=1, keepdims=True),
            jnp.sum(conv_out * conv_out, axis=1, keepdims=True),
        ),
        TP,
    )
    row_mean = channel_sums[0] / CONV_CH
    row_var = channel_sums[1] / CONV_CH - row_mean * row_mean
    activated = jax.nn.silu(
        (conv_out - row_mean) * lax.rsqrt(row_var + epsilon) * channel_gain
    ).astype(jnp.bfloat16)
    mixer_out = (
        by_axis(
            jnp.dot(activated, w_output, preferred_element_type=jnp.float32).astype(jnp.bfloat16),
            TP,
        )
        .astype(jnp.float32)
        .astype(jnp.bfloat16)
    )
    rows_b = expert_in.shape[0]
    width = expert_in.shape[1]
    experts = lax.axis_size("ep")
    capacity = 2 * rows_b * TOP_K // experts
    slot_share = capacity // lax.axis_size(TP)
    column = lax.axis_index(TP)
    normed_b = row_norm(expert_in, expert_gain).astype(jnp.bfloat16)
    raised = jnp.exp(route_scores)
    route_weights = raised / jnp.sum(raised, axis=1, keepdims=True)
    flat_ids = route_experts.reshape(-1)
    onehot = (flat_ids[:, None] == jnp.arange(experts, dtype=jnp.int32)[None, :]).astype(jnp.int32)
    slot_index = jnp.sum((jnp.cumsum(onehot, axis=0) - onehot) * onehot, axis=1)
    owner_row = jnp.arange(rows_b * TOP_K, dtype=jnp.int32) // TOP_K
    slot_table = (
        jnp.full((capacity * experts,), rows_b, jnp.int32)
        .at[slot_index * experts + flat_ids]
        .set(owner_row)
    )
    padded = jnp.concatenate([normed_b, jnp.zeros((1, width), jnp.bfloat16)], axis=0)
    gate_w = expert_gate[0]
    up_w = expert_up[0]
    down_w = expert_down[0]
    own_table = lax.dynamic_slice_in_dim(
        slot_table, column * slot_share * experts, slot_share * experts
    )
    sending = jnp.take(padded, own_table, axis=0).reshape(slot_share, experts, width)
    arrived = lax.all_to_all(sending, "ep", split_axis=1, concat_axis=1, tiled=True)
    block_rows = lax.all_gather(arrived, TP, axis=0, tiled=True)
    flat_rows = block_rows.reshape(block_rows.shape[0] * block_rows.shape[1], block_rows.shape[2])
    gate_e = jnp.minimum(
        jnp.dot(flat_rows, gate_w, preferred_element_type=jnp.float32), clamp_limit
    )
    up_e = jnp.clip(
        jnp.dot(flat_rows, up_w, preferred_element_type=jnp.float32), -clamp_limit, clamp_limit
    )
    hidden = (
        ((up_e + 1.0) * gate_e * jax.nn.sigmoid(swish_slope * gate_e))
        .astype(jnp.bfloat16)
        .reshape(block_rows.shape[0], block_rows.shape[1], gate_w.shape[1])
        .reshape(capacity * experts, gate_w.shape[1])
    )
    summed = lax.psum_scatter(
        jnp.dot(hidden, down_w, preferred_element_type=jnp.float32).astype(jnp.bfloat16),
        TP,
        scatter_dimension=0,
        tiled=True,
    )
    returned = lax.all_to_all(
        summed.reshape(slot_share, experts, width), "ep", split_axis=1, concat_axis=1, tiled=True
    )
    every_slot = lax.all_gather(returned, TP, axis=0, tiled=True).reshape(capacity * experts, width)
    picked = jnp.take(every_slot, slot_index * experts + flat_ids, axis=0)
    picked = picked.reshape(rows_b, TOP_K, width).astype(jnp.float32)
    expert_out = jnp.sum(picked * route_weights[:, :, None], axis=1).astype(jnp.bfloat16)
    return (mixer_out, expert_out)


def solution(mesh):
    split = Mesh(mesh.devices.reshape(mesh.shape["ep"], 8, 2), ("ep", "tp_0", "tp_1"))
    in_specs = (
        P("ep", None),
        P(),
        P(None, TP),
        P(None, TP),
        P(None, TP),
        P(TP),
        P(TP, None),
        P("ep", None),
        P(),
        P("ep", None),
        P("ep", None),
        P("ep", None, TP),
        P("ep", None, TP),
        P("ep", TP, None),
    )
    out_specs = (P("ep", None), P("ep", None))
    return jax.shard_map(local, mesh=split, in_specs=in_specs, out_specs=out_specs, check_vma=False)
```

profile of v0, /device:TPU:1, one launch (start us, length us, event | category | flops | bytes accessed | tf_op | source)
XLA Modules:
  0.0 251.4 jit_solution(10205323536202366580)
XLA Ops:
  8.0 0.0 copy-start
  8.0 0.0 all-gather.3.cloned.1.call-start
  8.1 0.9 copy.59
  9.0 0.1 eq.29
  9.1 0.1 eq.25
  9.2 0.1 reshape.133
  9.3 1.2 reduce-window.6
  10.5 0.2 slice_reduce_fusion
  10.7 0.1 fusion.34
  10.9 2.4 scatter_custom_fusion
  13.3 0.1 compare_and_fusion
  13.4 1.2 convert_reduce_fusion
  14.6 1.3 fusion.13
  16.0 0.1 broadcast_in_dim.45
  16.1 0.1 copy.65
  16.2 1.4 fusion.15
  17.6 0.7 gather_fusion
  18.4 0.0 copy-start.2
  18.4 0.3 broadcast_select_fusion
  18.7 24.8 %all_to_all.16 = bf16[2,32,2048]{2,0,1:T(2,128)(2,1)S(1)} all-to-all(bf16[2,32,2048]{2,0,1:T(2,128)(2,1)S(1)} %broadcast_select_fusion), channel_id=1, replica_groups=mesh['ep'=32,'tp_0'=8,'tp_1'=2] {'ep'}, dimensions={1} | all-to-all | bytes 524288 | tf_op jit(solution)/shard_map/all_to_all | solution.py:129
  43.6 0.8 copy.67
  44.3 0.0 all-gather.3.cloned.1.call-update
  44.4 0.0 reduce-scatter.2.cloned.1.call-start
  44.4 42.1 %all-gather.3.cloned.1.call-done = bf16[32,32,2048]{2,1,0:T(8,128)(2,1)} async-done(((bf16[2,32,2048]{2,1,0:T(8,128)(2,1)}), bf16[32,32,2048]{2,1,0:T(8,128)(2,1)}) %all-gather.3.cloned.1.call-update) | async-done | bytes 4194320 | tf_op jit(solution)/shard_map/all_gather | solution.py:130
  86.5 0.0 copy-done.8
  86.5 3.4 %convolution_minimum_fusion = f32[1024,128]{1,0:T(8,128)S(1)} fusion(bf16[1024,2048]{1,0:T(8,128)(2,1)} %bitcast.103, bf16[1,2048,128]{2,1,0:T(8,128)(2,1)S(1)} %copy-done.8), kind=kOutput, calls=%fused_computation.14 | convolution fusion | flops 537001984 | bytes 5242880 | tf_op jit(solution)/shard_map/dot_general | solution.py:133
  90.0 8.5 %convolution_convert_fusion = bf16[1024,2048]{1,0:T(8,128)(2,1)} fusion(f32[1024,128]{1,0:T(8,128)S(1)} %convolution_minimum_fusion, bf16[1024,2048]{1,0:T(8,128)(2,1)} %bitcast.104, bf16[1,128,2048]{2,1,0:T(8,128)(2,1)S(1)} %copy-done, bf16[1,2048,128]{2,1,0:T(8,128)(2,1)S(1)} %copy-done.2), kind=kOutput, calls=%fused_computation.4 | convolution fusion | flops 1077018624 | bytes 9961472 | tf_op jit(solution)/shard_map/dot_general | solution.py:145
  98.5 0.0 copy-start.4
  98.5 0.0 copy-start.3
  98.5 0.0 copy-start.7
  98.5 0.0 reduce-scatter.2.cloned.1.call-update
  98.5 0.0 copy-start.5
  98.6 0.0 copy-start.6
  98.6 0.0 all-reduce.4.cloned.1.call-start
  98.6 0.9 copy-done.1
  99.5 0.2 convert_reduce_fusion.1
  99.7 0.3 fusion.16
  100.0 0.4 fusion.80
  100.4 0.4 fusion.12
  100.8 0.1 slice.268
  100.9 3.1 %collective-permute-start = (bf16[30,96]{0,1:T(8,128)(2,1)S(1)}, bf16[30,96]{0,1:T(8,128)(2,1)S(1)}, u32[]{:S(2)}, u32[]{:S(2)}) collective-permute-start(bf16[30,96]{0,1:T(8,128)(2,1)S(1)} %slice.268), channel_id=1, source_target_pairs={{0,16},{16,32},{32,48},{48,64},{64,80},{80,96},{96,112},{112,128},... | collective-permute-start | bytes 17288 | tf_op jit(solution)/shard_map/ppermute | solution.py:19
  104.1 0.9 collective-permute-done
  104.9 0.9 fusion.82
  105.8 12.5 %all_to_all.17 = f32[16,1,256]{2,1,0:T(1,128)S(1)} all-to-all(f32[16,1,256]{2,1,0:T(1,128)S(1)} %broadcast_in_dim.42), channel_id=1, replica_groups=mesh['ep'=32,'tp_0'=8,'tp_1'=2] {'tp_0','tp_1'}, dimensions={0} | all-to-all | bytes 32768 | tf_op jit(solution)/shard_map/all_to_all | solution.py:24
  118.4 1.2 convolution_convert_fusion.1
  119.6 0.0 all-reduce.4.cloned.1.call-update
  119.6 0.0 all-gather.5.cloned.1.call-start
  119.6 42.9 %reduce-scatter.2.cloned.1.call-done = bf16[64,2048]{1,0:T(8,128)(2,1)} async-done(((bf16[1024,2048]{1,0:T(8,128)(2,1)}), bf16[64,2048]{1,0:T(8,128)(2,1)}) %reduce-scatter.2.cloned.1.call-update) | async-done | bytes 262160 | tf_op jit(solution)/shard_map/reduce_scatter | solution.py:144
  162.5 1.2 copy.68
  163.8 18.9 %all_to_all.18 = bf16[2,32,2048]{2,0,1:T(2,128)(2,1)S(1)} all-to-all(bf16[2,32,2048]{2,0,1:T(2,128)(2,1)S(1)} %copy.68), channel_id=1, replica_groups=mesh['ep'=32,'tp_0'=8,'tp_1'=2] {'ep'}, dimensions={1} | all-to-all | bytes 524288 | tf_op jit(solution)/shard_map/all_to_all | solution.py:150
  182.7 0.8 copy.69
  183.5 0.0 all-gather.5.cloned.1.call-update
  183.5 0.2 all-reduce.6.cloned.1.call-start
  183.7 0.1 mul.529
  183.8 0.1 copy.62
  183.9 0.1 copy.63
  184.1 0.1 copy.70
  184.2 9.5 %all-reduce.4.cloned.1.call-done = bf16[128,2048]{1,0:T(8,128)(2,1)} async-done(((bf16[128,2048]{1,0:T(8,128)(2,1)}), bf16[128,2048]{1,0:T(8,128)(2,1)}) %all-reduce.4.cloned.1.call-update) | async-done | bytes 524304 | tf_op jit(solution)/shard_map/psum | solution.py:43
  193.7 0.0 all-reduce.6.cloned.1.call-update
  193.8 32.8 %all-gather.5.cloned.1.call-done = bf16[32,32,2048]{2,1,0:T(8,128)(2,1)} async-done(((bf16[2,32,2048]{2,1,0:T(8,128)(2,1)}), bf16[32,32,2048]{2,1,0:T(8,128)(2,1)}) %all-gather.5.cloned.1.call-update) | async-done | bytes 4194320 | tf_op jit(solution)/shard_map/all_gather | solution.py:153
  226.6 7.1 %gather_fusion.1 = bf16[512,2048]{1,0:T(8,128)(2,1)S(1)} fusion(bf16[1024,2048]{1,0:T(8,128)(2,1)} %bitcast.102, s32[1024]{0:T(1024)S(1)} %pad_clamp_fusion), kind=kCustom, calls=%fused_computation.1 | custom fusion | bytes 4196352 | tf_op jit(solution)/shard_map/jit(_take)/gather | solution.py:154
  233.7 2.2 gather.15
  236.0 6.4 %multiply_reduce_fusion = bf16[128,2048]{1,0:T(8,128)(2,1)} fusion(f32[128,4]{1,0:T(8,128)S(1)} %copy.70, bf16[128,4,2048]{2,1,0:T(4,128)(2,1)} %gather.15, pred[128,4]{1,0:T(8,128)(4,1)S(1)} %copy.63), kind=kLoop, calls=%fused_computation.3 | loop fusion | flops 3932160 | bytes 2624000 | tf_op jit(solution)/shard_map/reduce_sum | solution.py:156
  242.4 1.9 copy.79
  (38 shorter events, 0.3 us)
Async XLA Ops:
  8.0 82.0 %copy-start = (bf16[1,128,2048]{2,1,0:T(8,128)(2,1)S(1)}, bf16[1,128,2048]{2,1,0:T(8,128)(2,1)}, u32[]{:S(2)}) copy-start(bf16[1,128,2048]{2,1,0:T(8,128)(2,1)} %param.27) | copy-start | bytes 1572868
  8.0 78.5 %copy-start.8 = (bf16[1,2048,128]{2,1,0:T(8,128)(2,1)S(1)}, bf16[1,2048,128]{2,1,0:T(8,128)(2,1)}, u32[]{:S(2)}) copy-start(bf16[1,2048,128]{2,1,0:T(8,128)(2,1)} %param.25) | copy-start | bytes 1572868
  8.0 78.5 %all-gather.3.cloned.1.call-start = ((), (), s32[]{:S(2)}) async-start(), calls=%async_computation.6 | async-start | bytes 4456448 | tf_op jit(solution)/shard_map/all_gather | solution.py:130
  18.4 71.6 %copy-start.2 = (bf16[1,2048,128]{2,1,0:T(8,128)(2,1)S(1)}, bf16[1,2048,128]{2,1,0:T(8,128)(2,1)}, u32[]{:S(2)}) copy-start(bf16[1,2048,128]{2,1,0:T(8,128)(2,1)} %param.26) | copy-start | bytes 1572868
  44.4 118.2 %reduce-scatter.2.cloned.1.call-start = ((), (), s32[]{:S(2)}) async-start(), calls=%async_computation.7 | async-start | bytes 4456448 | tf_op jit(solution)/shard_map/reduce_scatter | solution.py:144
  98.5 1.0 copy-start.1
  98.5 1.5 copy-start.9
  98.5 1.5 copy-start.11
  98.5 1.9 copy-start.10
  98.5 5.5 %copy-start.4 = (f32[31,96]{1,0:T(8,128)S(1)}, f32[31,96]{1,0:T(8,128)}, u32[]{:S(2)}) copy-start(f32[31,96]{1,0:T(8,128)} %param.18) | copy-start | bytes 35716
  98.5 19.9 %copy-start.3 = (bf16[96,2048]{1,0:T(8,128)(2,1)S(1)}, bf16[96,2048]{1,0:T(8,128)(2,1)}, u32[]{:S(2)}) copy-start(bf16[96,2048]{1,0:T(8,128)(2,1)} %param.20) | copy-start | bytes 1179652
  98.5 19.8 %copy-start.7 = (f32[96]{0:T(128)S(1)}, f32[96]{0:T(128)}, u32[]{:S(2)}) copy-start(f32[96]{0:T(128)} %param.19) | copy-start | bytes 1156
  98.5 85.3 %copy-start.5 = (s32[128,4]{0,1:T(4,128)S(1)}, s32[128,4]{0,1:T(4,128)}, u32[]{:S(2)}) copy-start(s32[128,4]{0,1:T(4,128)} %param.23) | copy-start | bytes 6148
  98.6 85.5 %copy-start.6 = (f32[128,4]{0,1:T(4,128)S(1)}, f32[128,4]{0,1:T(4,128)}, u32[]{:S(2)}) copy-start(f32[128,4]{0,1:T(4,128)} %param.24) | copy-start | bytes 6148
  98.6 95.1 %all-reduce.4.cloned.1.call-start = ((), (), s32[]{:S(2)}) async-start(), calls=%async_computation.4 | async-start | bytes 1048576 | tf_op jit(solution)/shard_map/psum | solution.py:43
  100.9 4.0 %collective-permute-start = (bf16[30,96]{0,1:T(8,128)(2,1)S(1)}, bf16[30,96]{0,1:T(8,128)(2,1)S(1)}, u32[]{:S(2)}, u32[]{:S(2)}) collective-permute-start(bf16[30,96]{0,1:T(8,128)(2,1)S(1)} %slice.268), channel_id=1, source_target_pairs={{0,16},{16,32},{32,48},{48,64},{64,80},{80,96},{96,112},{112,128},... | collective-permute-start | bytes 17288 | tf_op jit(solution)/shard_map/ppermute | solution.py:19
  119.6 107.0 %all-gather.5.cloned.1.call-start = ((), (), s32[]{:S(2)}) async-start(), calls=%async_computation.8 | async-start | bytes 4456448 | tf_op jit(solution)/shard_map/all_gather | solution.py:153
  183.5 58.9 %all-reduce.6.cloned.1.call-start = ((), (), s32[]{:S(2)}) async-start(), calls=%async_computation.5 | async-start | bytes 1048576 | tf_op jit(solution)/shard_map/psum | solution.py:43
Sparse Core Ops, SparseCore 0:
  44.5 42.0 all-gather.2
  98.7 63.8 reduce-scatter.1
  183.6 42.9 all-gather.4
Sparse Core Ops, SparseCore 1:
  119.7 74.0 all-reduce.3
  196.5 39.0 all-reduce.5
where the time goes:
time: 252 us; the launch traced here: 251 us
  waiting for transfers between devices  128 us (51%)
  blocking collectives  56.2 us (22%)
  local copies, waits for them, and re-layouts  20.4 us (8%)
  between operations  15.5 us (6%)
  matrix products  13.9 us (6%)
  other arithmetic  13.6 us (5%)
  starting transfers between devices  3.48 us (1%)
    reduce_scatter x1, waiting for transfers between devices, local(): lax.psum_scatter(jnp.dot(hidden, down_w, preferred_element_type=jnp.float...  42.9 us
    all_gather x1, waiting for transfers between devices, local(): block_rows = lax.all_gather(arrived, TP, axis=0, tiled=True)  42.1 us
    all_gather x1, waiting for transfers between devices, local(): lax.all_gather(returned, TP, axis=0, tiled=True)  32.8 us
    all_to_all x1, blocking collectives, local(): lax.all_to_all(sending, 'ep', split_axis=1, concat_axis=1, tiled=True)  24.8 us
    all_to_all x1, blocking collectives, local(): lax.all_to_all(summed.reshape(slot_share, experts, width), 'ep', split_ax...  18.9 us
    all_to_all x1, blocking collectives, sent_to_all(): return lax.all_to_all(copies, axis, split_axis=0, concat_axis=0, tiled=True)  12.5 us
    psum x2, waiting for transfers between devices, by_axis(): x = lax.psum(x, axis)  9.51 us
    gather x2, local copies, waits for them, and re-layouts, local(): picked = jnp.take(every_slot, slot_index * experts + flat_ids, axis=0)  9.37 us
  transfers between devices with their start and end apart: 6, of which 5 were waited for; matrix products, arithmetic and copies ran while one was open for 9% of the time, Pallas kernels for 0%

commit v1 on v0

--- a/solution.py
+++ b/solution.py
@@ -11,6 +11,11 @@
 epsilon = 1e-05
 clamp_limit = 7.0
 swish_slope = 1.702
+
+
+def gather_over(x, axis, d):
+    stack = jnp.stack([x] * lax.axis_size(axis))
+    return jnp.concatenate(lax.all_to_all(stack, axis, 0, 0), axis=d)
 
 
 def shifted(block, axis, distance):
@@ -150,7 +155,7 @@
     returned = lax.all_to_all(
         summed.reshape(slot_share, experts, width), "ep", split_axis=1, concat_axis=1, tiled=True
     )
-    every_slot = lax.all_gather(returned, TP, axis=0, tiled=True).reshape(capacity * experts, width)
+    every_slot = gather_over(returned, TP, 0).reshape(capacity * experts, width)
     picked = jnp.take(every_slot, slot_index * experts + flat_ids, axis=0)
     picked = picked.reshape(rows_b, TOP_K, width).astype(jnp.float32)
     expert_out = jnp.sum(picked * route_weights[:, :, None], axis=1).astype(jnp.bfloat16)

time: 252 us -> 363 us (1.44)
  waiting for transfers between devices: 128 us -> 243 us
  blocking collectives: 56.2 us -> 24.8 us
  starting transfers between devices: 3.48 us -> 27.2 us
    psum x2, waiting for transfers between devices: 9.51 us -> 127 us  [by_axis(): x = lax.psum(x, axis)]
    all_gather x1 -> x0, waiting for transfers between devices: 32.8 us -> none  [local(): lax.all_gather(returned, TP, axis=0, tiled=True)]
    all_to_all x2 -> x0, blocking collectives: 31.4 us -> none  [the longest x1 18.9 us: local(): lax.all_to_all(summed.reshape(slot_share, experts, width), 'ep', split_ax...]
    all_to_all x0 -> x3, starting transfers between devices: none -> 23.8 us  [the longest x1 9.88 us: sent_to_all(): return lax.all_to_all(copies, axis, split_axis=0, concat_axis=0, tiled=True)]
    all_to_all x0 -> x3, waiting for transfers between devices: none -> 16.8 us  [the longest x1 9.57 us: local(): lax.all_to_all(summed.reshape(slot_share, experts, width), 'ep', split_ax...]
    reduce_scatter x1, waiting for transfers between devices: 42.9 us -> 56.7 us  [local(): lax.psum_scatter(jnp.dot(hidden, down_w, preferred_element_type=jnp.float...]
  transfers between devices with their start and end apart: 6 -> 8, of which waited for: 5 -> 6; matrix products, arithmetic and copies ran while one was open for 9% -> 6% of each run, Pallas kernels for 0% -> 0%
where the time goes in v1:
time: 363 us; the launch traced here: 362 us
  waiting for transfers between devices  243 us (67%)
  starting transfers between devices  27.2 us (7%)
  blocking collectives  24.8 us (7%)
  local copies, waits for them, and re-layouts  23.6 us (7%)
  between operations  15.8 us (4%)
  matrix products  13.9 us (4%)
  other arithmetic  13.6 us (4%)
    psum x2, waiting for transfers between devices, by_axis(): x = lax.psum(x, axis)  127 us
    reduce_scatter x1, waiting for transfers between devices, local(): lax.psum_scatter(jnp.dot(hidden, down_w, preferred_element_type=jnp.float...  56.7 us
    all_gather x1, waiting for transfers between devices, local(): block_rows = lax.all_gather(arrived, TP, axis=0, tiled=True)  42.1 us
    all_to_all x1, blocking collectives, local(): lax.all_to_all(sending, 'ep', split_axis=1, concat_axis=1, tiled=True)  24.8 us
    all_to_all x1, starting transfers between devices, sent_to_all(): return lax.all_to_all(copies, axis, split_axis=0, concat_axis=0, tiled=True)  9.88 us
    all_to_all x1, waiting for transfers between devices, local(): lax.all_to_all(summed.reshape(slot_share, experts, width), 'ep', split_ax...  9.57 us
    gather x2, local copies, waits for them, and re-layouts, local(): picked = jnp.take(every_slot, slot_index * experts + flat_ids, axis=0)  9.37 us
    all_to_all x1, starting transfers between devices, local(): lax.all_to_all(summed.reshape(slot_share, experts, width), 'ep', split_ax...  9.1 us
  transfers between devices with their start and end apart: 8, of which 6 were waited for; matrix products, arithmetic and copies ran while one was open for 6% of the time, Pallas kernels for 0%

profile of v1, /device:TPU:1, one launch (start us, length us, event | category | flops | bytes accessed | tf_op | source)
XLA Modules:
  0.0 362.1 jit_solution(1157227760470907698)
XLA Ops:
  8.0 0.0 copy-start
  8.0 0.0 all-gather.2.cloned.1.call-start
  8.1 0.9 copy.59
  9.0 0.1 eq.29
  9.1 0.1 eq.25
  9.2 0.1 reshape.132
  9.3 1.2 reduce-window.6
  10.5 0.2 slice_reduce_fusion
  10.7 0.1 fusion.34
  10.9 2.4 scatter_custom_fusion
  13.3 0.1 compare_and_fusion
  13.4 1.2 convert_reduce_fusion
  14.6 1.3 fusion.13
  16.0 0.1 broadcast_in_dim.45
  16.1 0.1 copy.65
  16.2 1.4 fusion.15
  17.6 0.7 gather_fusion
  18.4 0.0 copy-start.2
  18.4 0.3 broadcast_select_fusion
  18.7 24.8 %all_to_all.21 = bf16[2,32,2048]{2,0,1:T(2,128)(2,1)S(1)} all-to-all(bf16[2,32,2048]{2,0,1:T(2,128)(2,1)S(1)} %broadcast_select_fusion), channel_id=1, replica_groups=mesh['ep'=32,'tp_0'=8,'tp_1'=2] {'ep'}, dimensions={1} | all-to-all | bytes 524288 | tf_op jit(solution)/shard_map/all_to_all | solution.py:134
  43.6 0.8 copy.67
  44.3 0.0 all-gather.2.cloned.1.call-update
  44.4 0.0 reduce-scatter.2.cloned.1.call-start
  44.4 42.1 %all-gather.2.cloned.1.call-done = bf16[32,32,2048]{2,1,0:T(8,128)(2,1)} async-done(((bf16[2,32,2048]{2,1,0:T(8,128)(2,1)}), bf16[32,32,2048]{2,1,0:T(8,128)(2,1)}) %all-gather.2.cloned.1.call-update) | async-done | bytes 4194320 | tf_op jit(solution)/shard_map/all_gather | solution.py:135
  86.5 3.4 convolution_minimum_fusion
  90.0 8.5 %convolution_convert_fusion = bf16[1024,2048]{1,0:T(8,128)(2,1)} fusion(f32[1024,128]{1,0:T(8,128)S(1)} %convolution_minimum_fusion, bf16[1024,2048]{1,0:T(8,128)(2,1)} %bitcast.103, bf16[1,128,2048]{2,1,0:T(8,128)(2,1)S(1)} %copy-done, bf16[1,2048,128]{2,1,0:T(8,128)(2,1)S(1)} %copy-done.2), kind=kOutput, calls=%fused_computation.4 | convolution fusion | flops 1077018624 | bytes 9961472 | tf_op jit(solution)/shard_map/dot_general | solution.py:150
  98.5 0.0 copy-start.4
  98.5 0.0 reduce-scatter.2.cloned.1.call-update
  98.5 1.0 copy-done.1
  99.5 0.2 convert_reduce_fusion.1
  99.7 0.3 fusion.16
  100.0 0.4 fusion.80
  100.4 0.4 fusion.12
  100.8 0.1 slice.268
  100.9 3.1 collective-permute-start
  104.1 56.7 %reduce-scatter.2.cloned.1.call-done = bf16[64,2048]{1,0:T(8,128)(2,1)} async-done(((bf16[1024,2048]{1,0:T(8,128)(2,1)}), bf16[64,2048]{1,0:T(8,128)(2,1)}) %reduce-scatter.2.cloned.1.call-update) | async-done | bytes 262160 | tf_op jit(solution)/shard_map/reduce_scatter | solution.py:149
  160.8 1.9 copy.68
  162.7 9.1 %all-to-all-start.2 = ((bf16[2,32,2048]{2,0,1:T(2,128)(2,1)}), bf16[2,32,2048]{2,0,1:T(2,128)(2,1)S(1)}, u32[]{:S(2)}, u32[]{:S(2)}) async-start(bf16[2,32,2048]{2,0,1:T(2,128)(2,1)} %copy.68), calls=%async_computation.3 | async-start | bytes 524288 | tf_op jit(solution)/shard_map/all_to_all | solution.py:155
  171.8 0.0 collective-permute-done
  171.8 0.9 fusion.82
  172.7 9.6 %all-to-all-done.2 = bf16[2,32,2048]{2,0,1:T(2,128)(2,1)S(1)} async-done(((bf16[2,32,2048]{2,0,1:T(2,128)(2,1)}), bf16[2,32,2048]{2,0,1:T(2,128)(2,1)S(1)}, u32[]{:S(2)}, u32[]{:S(2)}) %all-to-all-start.2) | async-done | bytes 262176 | tf_op jit(solution)/shard_map/all_to_all | solution.py:155
  182.3 0.6 broadcast_in_dim.42
  182.9 9.9 %all-to-all-start = ((f32[16,1,256]{2,1,0:T(1,128)}), f32[16,1,256]{2,1,0:T(1,128)S(1)}, u32[]{:S(2)}, u32[]{:S(2)}) async-start(f32[16,1,256]{2,1,0:T(1,128)} %broadcast_in_dim.42), calls=%async_computation | async-start | bytes 32768 | tf_op jit(solution)/shard_map/all_to_all | solution.py:29
  192.8 0.1 copy.69
  192.9 7.3 %all-to-all-done = f32[16,1,256]{2,1,0:T(1,128)S(1)} async-done(((f32[16,1,256]{2,1,0:T(1,128)}), f32[16,1,256]{2,1,0:T(1,128)S(1)}, u32[]{:S(2)}, u32[]{:S(2)}) %all-to-all-start) | async-done | bytes 16416 | tf_op jit(solution)/shard_map/all_to_all | solution.py:29
  200.1 2.5 stack.2
  202.6 4.8 %all-to-all-start.3 = ((bf16[16,2,32,2048]{3,2,1,0:T(8,128)(2,1)}), bf16[16,2,32,2048]{3,2,1,0:T(8,128)(2,1)}, u32[]{:S(2)}, u32[]{:S(2)}) async-start(bf16[16,2,32,2048]{3,2,1,0:T(8,128)(2,1)} %stack.2), calls=%async_computation.4 | async-start | bytes 8388608 | tf_op jit(solution)/shard_map/all_to_all | solution.py:18
  207.4 0.0 all-reduce.4.cloned.1.call-start
  207.5 0.1 mul.529
  207.6 0.1 copy.62
  207.6 0.1 reduce_sum.94
  207.7 1.2 convolution_convert_fusion.1
  208.9 0.0 all-reduce.4.cloned.1.call-update
  208.9 0.2 all-reduce.6.cloned.1.call-start
  209.2 0.1 copy.63
  209.4 0.1 copy.70
  209.5 106.4 %all-reduce.4.cloned.1.call-done = bf16[128,2048]{1,0:T(8,128)(2,1)} async-done(((bf16[128,2048]{1,0:T(8,128)(2,1)}), bf16[128,2048]{1,0:T(8,128)(2,1)}) %all-reduce.4.cloned.1.call-update) | async-done | bytes 524304 | tf_op jit(solution)/shard_map/psum | solution.py:48
  315.9 0.0 all-reduce.6.cloned.1.call-update
  316.0 0.0 all-to-all-done.3
  316.0 7.1 %gather_fusion.1 = bf16[512,2048]{1,0:T(8,128)(2,1)S(1)} fusion(bf16[1024,2048]{1,0:T(8,128)(2,1)} %bitcast.40, s32[1024]{0:T(1024)S(1)} %pad_clamp_fusion), kind=kCustom, calls=%fused_computation.1 | custom fusion | bytes 4196352 | tf_op jit(solution)/shard_map/jit(_take)/gather | solution.py:159
  323.1 2.2 gather.15
  325.3 6.4 %multiply_reduce_fusion = bf16[128,2048]{1,0:T(8,128)(2,1)} fusion(f32[128,4]{1,0:T(8,128)S(1)} %copy.70, bf16[128,4,2048]{2,1,0:T(4,128)(2,1)} %gather.15, pred[128,4]{1,0:T(8,128)(4,1)S(1)} %copy.63), kind=kLoop, calls=%fused_computation.3 | loop fusion | flops 3932160 | bytes 2624000 | tf_op jit(solution)/shard_map/reduce_sum | solution.py:161
  331.8 21.0 %all-reduce.6.cloned.1.call-done = bf16[128,2048]{1,0:T(8,128)(2,1)} async-done(((bf16[128,2048]{1,0:T(8,128)(2,1)}), bf16[128,2048]{1,0:T(8,128)(2,1)}) %all-reduce.6.cloned.1.call-update) | async-done | bytes 524304 | tf_op jit(solution)/shard_map/psum | solution.py:48
  352.8 1.9 copy.79
  (40 shorter events, 0.3 us)
Async XLA Ops:
  8.0 82.0 %copy-start = (bf16[1,128,2048]{2,1,0:T(8,128)(2,1)S(1)}, bf16[1,128,2048]{2,1,0:T(8,128)(2,1)}, u32[]{:S(2)}) copy-start(bf16[1,128,2048]{2,1,0:T(8,128)(2,1)} %param.27) | copy-start | bytes 1572868
  8.0 78.5 %copy-start.8 = (bf16[1,2048,128]{2,1,0:T(8,128)(2,1)S(1)}, bf16[1,2048,128]{2,1,0:T(8,128)(2,1)}, u32[]{:S(2)}) copy-start(bf16[1,2048,128]{2,1,0:T(8,128)(2,1)} %param.25) | copy-start | bytes 1572868
  8.0 78.5 %all-gather.2.cloned.1.call-start = ((), (), s32[]{:S(2)}) async-start(), calls=%async_computation.7 | async-start | bytes 4456448 | tf_op jit(solution)/shard_map/all_gather | solution.py:135
  18.4 71.6 %copy-start.2 = (bf16[1,2048,128]{2,1,0:T(8,128)(2,1)S(1)}, bf16[1,2048,128]{2,1,0:T(8,128)(2,1)}, u32[]{:S(2)}) copy-start(bf16[1,2048,128]{2,1,0:T(8,128)(2,1)} %param.26) | copy-start | bytes 1572868
  44.4 116.4 %reduce-scatter.2.cloned.1.call-start = ((), (), s32[]{:S(2)}) async-start(), calls=%async_computation.8 | async-start | bytes 4456448 | tf_op jit(solution)/shard_map/reduce_scatter | solution.py:149
  98.5 1.0 copy-start.1
  98.5 1.5 copy-start.9
  98.5 1.5 copy-start.11
  98.5 1.9 copy-start.10
  98.5 5.5 %copy-start.4 = (f32[31,96]{1,0:T(8,128)S(1)}, f32[31,96]{1,0:T(8,128)}, u32[]{:S(2)}) copy-start(f32[31,96]{1,0:T(8,128)} %param.18) | copy-start | bytes 35716
  100.9 70.9 %collective-permute-start = (bf16[30,96]{0,1:T(8,128)(2,1)S(1)}, bf16[30,96]{0,1:T(8,128)(2,1)S(1)}, u32[]{:S(2)}, u32[]{:S(2)}) collective-permute-start(bf16[30,96]{0,1:T(8,128)(2,1)S(1)} %slice.268), channel_id=1, source_target_pairs={{0,16},{16,32},{32,48},{48,64},{64,80},{80,96},{96,112},{112,128},... | collective-permute-start | bytes 17288 | tf_op jit(solution)/shard_map/ppermute | solution.py:24
  162.7 19.6 %all-to-all-start.2 = ((bf16[2,32,2048]{2,0,1:T(2,128)(2,1)}), bf16[2,32,2048]{2,0,1:T(2,128)(2,1)S(1)}, u32[]{:S(2)}, u32[]{:S(2)}) async-start(bf16[2,32,2048]{2,0,1:T(2,128)(2,1)} %copy.68), calls=%async_computation.3 | async-start | bytes 524288 | tf_op jit(solution)/shard_map/all_to_all | solution.py:155
  182.9 17.2 %all-to-all-start = ((f32[16,1,256]{2,1,0:T(1,128)}), f32[16,1,256]{2,1,0:T(1,128)S(1)}, u32[]{:S(2)}, u32[]{:S(2)}) async-start(f32[16,1,256]{2,1,0:T(1,128)} %broadcast_in_dim.42), calls=%async_computation | async-start | bytes 32768 | tf_op jit(solution)/shard_map/all_to_all | solution.py:29
  202.6 5.1 %copy-start.3 = (bf16[96,2048]{1,0:T(8,128)(2,1)S(1)}, bf16[96,2048]{1,0:T(8,128)(2,1)}, u32[]{:S(2)}) copy-start(bf16[96,2048]{1,0:T(8,128)(2,1)} %param.20) | copy-start | bytes 1179652
  202.6 5.1 %copy-start.7 = (f32[96]{0:T(128)S(1)}, f32[96]{0:T(128)}, u32[]{:S(2)}) copy-start(f32[96]{0:T(128)} %param.19) | copy-start | bytes 1156
  202.6 6.6 %copy-start.5 = (s32[128,4]{0,1:T(4,128)S(1)}, s32[128,4]{0,1:T(4,128)}, u32[]{:S(2)}) copy-start(s32[128,4]{0,1:T(4,128)} %param.23) | copy-start | bytes 6148
  202.6 6.7 %copy-start.6 = (f32[128,4]{0,1:T(4,128)S(1)}, f32[128,4]{0,1:T(4,128)}, u32[]{:S(2)}) copy-start(f32[128,4]{0,1:T(4,128)} %param.24) | copy-start | bytes 6148
  202.6 113.3 %all-to-all-start.3 = ((bf16[16,2,32,2048]{3,2,1,0:T(8,128)(2,1)}), bf16[16,2,32,2048]{3,2,1,0:T(8,128)(2,1)}, u32[]{:S(2)}, u32[]{:S(2)}) async-start(bf16[16,2,32,2048]{3,2,1,0:T(8,128)(2,1)} %stack.2), calls=%async_computation.4 | async-start | bytes 8388608 | tf_op jit(solution)/shard_map/all_to_all | solution.py:18
  207.4 108.5 %all-reduce.4.cloned.1.call-start = ((), (), s32[]{:S(2)}) async-start(), calls=%async_computation.5 | async-start | bytes 1048576 | tf_op jit(solution)/shard_map/psum | solution.py:48
  208.9 143.8 %all-reduce.6.cloned.1.call-start = ((), (), s32[]{:S(2)}) async-start(), calls=%async_computation.6 | async-start | bytes 1048576 | tf_op jit(solution)/shard_map/psum | solution.py:48
Sparse Core Ops, SparseCore 0:
  44.5 42.0 all-gather.1
  98.6 62.0 reduce-scatter.1
Sparse Core Ops, SparseCore 1:
  210.8 105.1 all-reduce.3
  318.7 34.0 all-reduce.5
